TPU v7x, 32 devices: a whole 2x2x4 slice. The times are simulated.
32 devices in a mesh: ep: 8 (over z, x), tp: 4 (over y, core).
Axes of the slice: x: 2, y: 2, z: 4, core: 2. Of those that a mesh axis runs over, the one named last changes fastest.
Arguments:
- hidden_in: bfloat16 [256, 4096], P('ep'), may hold values from -6 to 6
- norm_gain: float32 [4096], replicated, may hold values from 0.1 to 1.9
- group_ids: int32 [256], P('ep'), may hold values from 0 to 1, as said below
- inner_ids: int32 [256, 4], P('ep'), may hold values from 0 to 7, as said below
- group_prob: float32 [256], P('ep'), may hold values from 0.25 to 1
- expert_prob: float32 [256, 4], P('ep'), may hold values from 0.1 to 1
- w_gate: bfloat16 [16, 4096, 1024], P('ep', None, 'tp'), may hold values from -0.09375 to 0.09375
- w_up: bfloat16 [16, 4096, 1024], P('ep', None, 'tp'), may hold values from -0.09375 to 0.09375
- w_down: bfloat16 [16, 1024, 4096], P('ep', None, 'tp'), may hold values from -0.1875 to 0.1875
Outputs:
- moe_out: bfloat16 [256, 4096], P('ep', 'tp')
Inputs may be any that keep to these rules, and one draw needn't show every extreme that they name: `group_ids`: among the 32 tokens of one index of ep no group is named by more than 16 tokens; one group is named by exactly 16 of them, and all of these name one common expert of it. `inner_ids`: each row names 4 different experts of the token's group.
All inputs are finite; a program needn't handle non-finite values.
Results may differ from a plain program's by a relative error of at most 0.0069.
Values may be sent and summed in bfloat16 or wider, within the bound.
No kernel may reach another device: no remote copies, remote signals or barrier semaphores. Data moves between devices by JAX's collectives and lax.ppermute only.
A program may use at most 64 MiB of HBM per device.

v0:
```python
import jax
import jax.numpy as jnp
from jax import lax
from jax.sharding import PartitionSpec as P

EPG = 8
EPS = 1e-06


def expert_block(token_rows, weights, w_gate, w_up, w_down):
    gate_proj = jnp.einsum("rd,edh->erh", token_rows, w_gate, preferred_element_type=jnp.float32)
    up_proj = jnp.einsum("rd,edh->erh", token_rows, w_up, preferred_element_type=jnp.float32)
    activation = (jax.nn.silu(gate_proj) * up_proj * weights.T[:, :, None]).astype(jnp.bfloat16)
    return jnp.einsum(
        "erh,ehd->rd",
        lax.all_gather(activation, "tp", axis=2, tiled=True),
        w_down,
        preferred_element_type=jnp.float32,
    )


def on_device(
    hidden_in, norm_gain, group_ids, inner_ids, group_prob, expert_prob, w_gate, w_up, w_down
):
    widened = hidden_in.astype(jnp.float32)
    normed = (
        widened * lax.rsqrt(jnp.mean(widened * widened, axis=-1, keepdims=True) + EPS) * norm_gain
    ).astype(jnp.bfloat16)
    ep_count = lax.axis_size("ep")
    local_count = w_gate.shape[0]
    expert_count = local_count * ep_count
    tok_rows = normed.shape[0]
    expert_ids = group_ids[:, None] * EPG + inner_ids
    scaled = group_prob[:, None] * expert_prob
    matches = (expert_ids[:, :, None] == jnp.arange(expert_count)[None, None, :]).astype(
        jnp.float32
    )
    route_dense = jnp.sum(matches * scaled[:, :, None], axis=1)
    capacity = tok_rows // 2
    owners = expert_ids // local_count
    routed = jnp.any(owners[:, :, None] == jnp.arange(ep_count)[None, None, :], axis=1)
    slot_index = jnp.cumsum(routed.astype(jnp.int32), axis=0) - 1
    hit_slot = slot_index.T[:, None, :] == jnp.arange(capacity)[None, :, None]
    dispatch = (routed.T[:, None, :] & hit_slot).astype(jnp.float32)
    send_rows = jnp.einsum(
        "psr,rd->psd", dispatch.astype(jnp.bfloat16), normed, preferred_element_type=jnp.float32
    ).astype(jnp.bfloat16)
    send_weights = jnp.einsum(
        "psr,rpe->pse",
        dispatch,
        route_dense.reshape(tok_rows, ep_count, local_count),
        precision=lax.Precision.HIGHEST,
    )
    got_rows = lax.all_to_all(send_rows, "ep", split_axis=0, concat_axis=0, tiled=True)
    got_weights = lax.all_to_all(send_weights, "ep", split_axis=0, concat_axis=0, tiled=True)
    partial_value = expert_block(
        got_rows.reshape(ep_count * capacity, got_rows.shape[2]),
        got_weights.reshape(ep_count * capacity, local_count),
        w_gate,
        w_up,
        w_down,
    )
    returned = lax.all_to_all(
        partial_value.reshape(ep_count, capacity, partial_value.shape[1]),
        "ep",
        split_axis=0,
        concat_axis=0,
        tiled=True,
    )
    combined = jnp.einsum("psr,psd->rd", dispatch, returned, precision=lax.Precision.HIGHEST)
    return combined.astype(jnp.bfloat16)


def solution(mesh):
    placed = (
        P("ep", None),
        P(),
        P("ep"),
        P("ep", None),
        P("ep"),
        P("ep", None),
        P("ep", None, "tp"),
        P("ep", None, "tp"),
        P("ep", None, "tp"),
    )
    return jax.shard_map(
        on_device, mesh=mesh, in_specs=placed, out_specs=P("ep", "tp"), check_vma=False
    )
```

profile of v0, /device:TPU:0, one launch (start us, length us, event | category | flops | bytes accessed | tf_op | source)
XLA Modules:
  0.0 76.7 jit_solution(13382884557020373992)
XLA Ops:
  0.0 0.7 broadcast_multiply_fusion.1
  0.7 0.7 add_select_fusion
  1.4 0.1 copy.21
  1.4 0.1 reduce_window_sum.11
  1.5 0.1 copy.22
  1.6 0.7 broadcast_multiply_fusion
  2.3 0.8 %fusion.13 = f32[8,16,2]{1,2,0:T(2,128)} fusion(f32[32,8,2]{0,2,1:T(2,128)S(1)} %bitcast.44, s32[8,32]{1,0:T(8,128)S(1)} %copy.22, pred[8,32]{1,0:T(8,128)(4,1)S(1)} %bitcast.41), kind=kOutput, calls=%fused_computation.19 | convolution fusion | flops 106496 | bytes 4352 | tf_op jit(solution)/shard_map/psr,rpe->pse/dot_general | solution.py:48
  3.1 7.3 %all-to-all-start.1 = ((f32[8,16,2]{1,2,0:T(2,128)}), f32[8,16,2]{1,2,0:T(2,128)S(1)}, u32[]{:S(2)}, u32[]{:S(2)}) async-start(f32[8,16,2]{1,2,0:T(2,128)} %fusion.13), calls=%async_computation.1 | async-start | bytes 16384 | tf_op jit(solution)/shard_map/all_to_all | solution.py:55
  10.3 1.1 %fusion.4 = f32[32]{0:T(128)S(1)} fusion(bf16[32,4096]{1,0:T(8,128)(2,1)} %param.9), kind=kLoop, calls=%fused_computation.10 | loop fusion | flops 393184 | bytes 262272 | tf_op jit(solution)/shard_map/reduce_sum | solution.py:27
  11.5 2.4 %convolution_convert_fusion = bf16[8,16,4096]{2,1,0:T(8,128)(2,1)} fusion(bf16[32,4096]{1,0:T(8,128)(2,1)} %param.9, f32[4096]{0:T(1024)} %param.10, f32[32]{0:T(128)S(1)} %add_rsqrt_fusion, s32[8,32]{1,0:T(8,128)S(1)} %copy.22, pred[8,32]{1,0:T(8,128)(4,1)S(1)} %bitcast.42), kind=kOutput, calls=%fused_computation | convolution fusion | flops 34619392 | bytes 1328512 | tf_op jit(solution)/shard_map/psr,rd->psd/dot_general | solution.py:45
  13.9 3.0 %all-to-all-done.1 = f32[8,16,2]{1,2,0:T(2,128)S(1)} async-done(((f32[8,16,2]{1,2,0:T(2,128)}), f32[8,16,2]{1,2,0:T(2,128)S(1)}, u32[]{:S(2)}, u32[]{:S(2)}) %all-to-all-start.1) | async-done | bytes 1056 | tf_op jit(solution)/shard_map/all_to_all | solution.py:55
  16.9 3.6 %all-to-all-start = ((bf16[8,16,4096]{2,1,0:T(8,128)(2,1)}), bf16[8,16,4096]{2,1,0:T(8,128)(2,1)S(1)}, u32[]{:S(2)}, u32[]{:S(2)}) async-start(bf16[8,16,4096]{2,1,0:T(8,128)(2,1)} %convolution_convert_fusion), calls=%async_computation | async-start | bytes 2097152 | tf_op jit(solution)/shard_map/all_to_all | solution.py:54
  20.4 0.1 reshape.32
  20.5 24.8 %all-to-all-done = bf16[8,16,4096]{2,1,0:T(8,128)(2,1)S(1)} async-done(((bf16[8,16,4096]{2,1,0:T(8,128)(2,1)}), bf16[8,16,4096]{2,1,0:T(8,128)(2,1)S(1)}, u32[]{:S(2)}, u32[]{:S(2)}) %all-to-all-start) | async-done | bytes 1048608 | tf_op jit(solution)/shard_map/all_to_all | solution.py:54
  45.3 0.0 copy-start.1
  45.3 3.0 %convolution_bitcast_fusion.1 = f32[2,128,256]{2,1,0:T(8,128)S(1)} fusion(bf16[128,4096,1]{1,0,2:T(8,128)(2,1)S(1)} %bitcast.38, bf16[2,4096,256]{2,1,0:T(8,128)(2,1)} %param.15), kind=kOutput, calls=%fused_computation.2 | convolution fusion | flops 536870912 | bytes 5505024 | tf_op jit(solution)/shard_map/rd,edh->erh/dot_general | solution.py:11
  48.4 0.0 copy-start
  48.4 0.4 copy-done.1
  48.8 0.8 fusion.2
  49.5 7.3 %all_gather.3 = bf16[2,128,1024]{2,1,0:T(8,128)(2,1)S(1)} all-gather(bf16[2,128,256]{2,1,0:T(8,128)(2,1)S(1)} %fusion.2), channel_id=1, replica_groups=mesh['ep'=8,'tp'=4] {'tp'}, dimensions={2}, use_global_device_ids=true | all-gather | bytes 655360 | tf_op jit(solution)/shard_map/all_gather | solution.py:16
  56.9 0.0 copy-done
  56.9 0.7 fusion.24
  57.6 18.2 %all_to_all.15 = f32[8,16,1024]{2,1,0:T(8,128)S(1)} all-to-all(f32[8,16,1024]{2,1,0:T(8,128)S(1)} %bitcast.40), channel_id=1, replica_groups=mesh['ep'=8,'tp'=4] {'ep'}, dimensions={0} | all-to-all | bytes 1048576 | tf_op jit(solution)/shard_map/all_to_all | solution.py:63
  75.8 0.9 %fusion.3 = bf16[32,1024]{1,0:T(8,128)(2,1)} fusion(f32[8,16,1024]{2,1,0:T(8,128)S(1)} %all_to_all.15, s32[8,32]{1,0:T(8,128)S(1)} %copy.22, pred[8,32]{1,0:T(8,128)(4,1)S(1)} %bitcast.43), kind=kOutput, calls=%fused_computation.7 | convolution fusion | flops 50372608 | bytes 591104 | tf_op jit(solution)/shard_map/psr,psd->rd/dot_general | solution.py:70
  (6 shorter events, 0.0 us)
Async XLA Ops:
  3.1 13.8 %all-to-all-start.1 = ((f32[8,16,2]{1,2,0:T(2,128)}), f32[8,16,2]{1,2,0:T(2,128)S(1)}, u32[]{:S(2)}, u32[]{:S(2)}) async-start(f32[8,16,2]{1,2,0:T(2,128)} %fusion.13), calls=%async_computation.1 | async-start | bytes 16384 | tf_op jit(solution)/shard_map/all_to_all | solution.py:55
  16.9 28.5 %all-to-all-start = ((bf16[8,16,4096]{2,1,0:T(8,128)(2,1)}), bf16[8,16,4096]{2,1,0:T(8,128)(2,1)S(1)}, u32[]{:S(2)}, u32[]{:S(2)}) async-start(bf16[8,16,4096]{2,1,0:T(8,128)(2,1)} %convolution_convert_fusion), calls=%async_computation | async-start | bytes 2097152 | tf_op jit(solution)/shard_map/all_to_all | solution.py:54
  45.3 3.4 %copy-start.1 = (bf16[2,4096,256]{2,1,0:T(8,128)(2,1)S(1)}, bf16[2,4096,256]{2,1,0:T(8,128)(2,1)}, u32[]{:S(2)}) copy-start(bf16[2,4096,256]{2,1,0:T(8,128)(2,1)} %param.16) | copy-start | bytes 12582916
  48.4 8.5 %copy-start = (bf16[2,1024,1024]{2,1,0:T(8,128)(2,1)S(1)}, bf16[2,1024,1024]{2,1,0:T(8,128)(2,1)}, u32[]{:S(2)}) copy-start(bf16[2,1024,1024]{2,1,0:T(8,128)(2,1)} %param.17) | copy-start | bytes 12582916
where the time goes:
time: 77.1 us; the launch traced here: 76.7 us
  waiting for transfers between devices  27.8 us (36%)
  blocking collectives  25.5 us (33%)
  starting transfers between devices  10.8 us (14%)
  matrix products  8.68 us (11%)
  other arithmetic  3.25 us (4%)
    all_to_all x1, waiting for transfers between devices, on_device(): lax.all_to_all(send_rows, 'ep', split_axis=0, concat_axis=0, tiled=True)  24.8 us
    all_to_all x1, blocking collectives, on_device(): lax.all_to_all(partial_value.reshape(ep_count, capacity, partial_value.sh...  18.2 us
    all_gather x1, blocking collectives, expert_block(): lax.all_gather(activation, 'tp', axis=2, tiled=True)  7.33 us
    all_to_all x1, starting transfers between devices, on_device(): lax.all_to_all(send_weights, 'ep', split_axis=0, concat_axis=0, tiled=True)  7.28 us
    all_to_all x1, starting transfers between devices, on_device(): lax.all_to_all(send_rows, 'ep', split_axis=0, concat_axis=0, tiled=True)  3.56 us
    dot_general x1, matrix products, expert_block(): jnp.einsum('rd,edh->erh', token_rows, w_gate, preferred_element_type=jnp....  3.04 us
    all_to_all x1, waiting for transfers between devices, on_device(): lax.all_to_all(send_weights, 'ep', split_axis=0, concat_axis=0, tiled=True)  2.97 us
    dot_general x1, matrix products, on_device(): jnp.einsum('psr,rd->psd', dispatch.astype(jnp.bfloat16), normed, preferre...  2.44 us
  transfers between devices with their start and end apart: 2, of which 2 were waited for; matrix products, arithmetic and copies ran while one was open for 5% of the time, Pallas kernels for 0%

commit v1 on v0

--- a/solution.py
+++ b/solution.py
@@ -7,15 +7,32 @@
 EPS = 1e-06
 
 
+def ring_product(shard, axis, dim, contribution):
+    count, mine = (lax.axis_size(axis), lax.axis_index(axis))
+    behind = [(i, (i - 1) % count) for i in range(count)]
+    extent = shard.shape[dim]
+    carried = shard
+    total = contribution(carried, mine * extent)
+    for turn in range(1, count):
+        carried = lax.ppermute(carried, axis, behind)
+        total = total + contribution(carried, (mine + turn) % count * extent)
+    return total
+
+
 def expert_block(token_rows, weights, w_gate, w_up, w_down):
     gate_proj = jnp.einsum("rd,edh->erh", token_rows, w_gate, preferred_element_type=jnp.float32)
     up_proj = jnp.einsum("rd,edh->erh", token_rows, w_up, preferred_element_type=jnp.float32)
     activation = (jax.nn.silu(gate_proj) * up_proj * weights.T[:, :, None]).astype(jnp.bfloat16)
-    return jnp.einsum(
-        "erh,ehd->rd",
-        lax.all_gather(activation, "tp", axis=2, tiled=True),
-        w_down,
-        preferred_element_type=jnp.float32,
+    return ring_product(
+        activation,
+        "tp",
+        2,
+        lambda part, at: jnp.einsum(
+            "erh,ehd->rd",
+            part,
+            lax.dynamic_slice_in_dim(w_down, at, part.shape[2], axis=1),
+            preferred_element_type=jnp.float32,
+        ),
     )
 
 

time: 77.1 us -> 82.3 us (1.067)
  blocking collectives: 25.5 us -> 19.7 us
  waiting for transfers between devices: 27.8 us -> 33.3 us
  starting transfers between devices: 10.8 us -> 14.6 us
  local copies, waits for them, and re-layouts: 0.62 us -> 1.68 us
    all_gather x1 -> x0, blocking collectives: 7.33 us -> none  [expert_block(): lax.all_gather(activation, 'tp', axis=2, tiled=True)]
    ppermute x0 -> x3, waiting for transfers between devices: none -> 5.54 us  [ring_product(): carried = lax.ppermute(carried, axis, behind)]
    ppermute x0 -> x3, starting transfers between devices: none -> 3.8 us  [ring_product(): carried = lax.ppermute(carried, axis, behind)]
    all_to_all x1, blocking collectives: 18.2 us -> 19.7 us  [on_device(): lax.all_to_all(partial_value.reshape(ep_count, capacity, partial_value.sh...]
    unnamed x4, local copies, waits for them, and re-layouts: 0.39 us -> 1.45 us
  transfers between devices with their start and end apart: 2 -> 5, of which waited for: 2 -> 5; matrix products, arithmetic and copies ran while one was open for 5% -> 6% of each run, Pallas kernels for 0% -> 0%
where the time goes in v1:
time: 82.3 us; the launch traced here: 81.9 us
  waiting for transfers between devices  33.3 us (40%)
  blocking collectives  19.7 us (24%)
  starting transfers between devices  14.6 us (18%)
  matrix products  9.2 us (11%)
  other arithmetic  3.25 us (4%)
  local copies, waits for them, and re-layouts  1.68 us (2%)
    all_to_all x1, waiting for transfers between devices, on_device(): lax.all_to_all(send_rows, 'ep', split_axis=0, concat_axis=0, tiled=True)  24.8 us
    all_to_all x1, blocking collectives, on_device(): lax.all_to_all(partial_value.reshape(ep_count, capacity, partial_value.sh...  19.7 us
    all_to_all x1, starting transfers between devices, on_device(): lax.all_to_all(send_weights, 'ep', split_axis=0, concat_axis=0, tiled=True)  7.28 us
    ppermute x3, waiting for transfers between devices, ring_product(): carried = lax.ppermute(carried, axis, behind)  5.54 us
    ppermute x3, starting transfers between devices, ring_product(): carried = lax.ppermute(carried, axis, behind)  3.8 us
    all_to_all x1, starting transfers between devices, on_device(): lax.all_to_all(send_rows, 'ep', split_axis=0, concat_axis=0, tiled=True)  3.56 us
    dot_general x1, matrix products, expert_block(): jnp.einsum('rd,edh->erh', token_rows, w_gate, preferred_element_type=jnp....  3.04 us
    all_to_all x1, waiting for transfers between devices, on_device(): lax.all_to_all(send_weights, 'ep', split_axis=0, concat_axis=0, tiled=True)  2.97 us
  transfers between devices with their start and end apart: 5, of which 5 were waited for; matrix products, arithmetic and copies ran while one was open for 6% of the time, Pallas kernels for 0%

profile of v1, /device:TPU:0, one launch (start us, length us, event | category | flops | bytes accessed | tf_op | source)
XLA Modules:
  0.0 81.9 jit_solution(4650236980277306266)
XLA Ops:
  0.0 0.7 broadcast_multiply_fusion.1
  0.7 0.7 add_select_fusion
  1.4 0.1 copy.21
  1.4 0.1 reduce_window_sum.11
  1.5 0.1 copy.22
  1.6 0.7 broadcast_multiply_fusion
  2.3 0.8 fusion.20
  3.1 7.3 %all-to-all-start.1 = ((f32[8,16,2]{1,2,0:T(2,128)}), f32[8,16,2]{1,2,0:T(2,128)S(1)}, u32[]{:S(2)}, u32[]{:S(2)}) async-start(f32[8,16,2]{1,2,0:T(2,128)} %fusion.20), calls=%async_computation.1 | async-start | bytes 16384 | tf_op jit(solution)/shard_map/all_to_all | solution.py:72
  10.3 1.1 %fusion.11 = f32[32]{0:T(128)S(1)} fusion(bf16[32,4096]{1,0:T(8,128)(2,1)} %param.9), kind=kLoop, calls=%fused_computation.21 | loop fusion | flops 393184 | bytes 262272 | tf_op jit(solution)/shard_map/reduce_sum | solution.py:44
  11.5 2.4 %convolution_convert_fusion = bf16[8,16,4096]{2,1,0:T(8,128)(2,1)} fusion(bf16[32,4096]{1,0:T(8,128)(2,1)} %param.9, f32[4096]{0:T(1024)} %param.10, f32[32]{0:T(128)S(1)} %add_rsqrt_fusion, s32[8,32]{1,0:T(8,128)S(1)} %copy.22, pred[8,32]{1,0:T(8,128)(4,1)S(1)} %bitcast.56), kind=kOutput, calls=%fused_computation | convolution fusion | flops 34619392 | bytes 1328512 | tf_op jit(solution)/shard_map/psr,rd->psd/dot_general | solution.py:62
  13.9 3.0 %all-to-all-done.1 = f32[8,16,2]{1,2,0:T(2,128)S(1)} async-done(((f32[8,16,2]{1,2,0:T(2,128)}), f32[8,16,2]{1,2,0:T(2,128)S(1)}, u32[]{:S(2)}, u32[]{:S(2)}) %all-to-all-start.1) | async-done | bytes 1056 | tf_op jit(solution)/shard_map/all_to_all | solution.py:72
  16.9 3.6 %all-to-all-start = ((bf16[8,16,4096]{2,1,0:T(8,128)(2,1)}), bf16[8,16,4096]{2,1,0:T(8,128)(2,1)S(1)}, u32[]{:S(2)}, u32[]{:S(2)}) async-start(bf16[8,16,4096]{2,1,0:T(8,128)(2,1)} %convolution_convert_fusion), calls=%async_computation | async-start | bytes 2097152 | tf_op jit(solution)/shard_map/all_to_all | solution.py:71
  20.5 0.1 reshape.32
  20.6 24.8 %all-to-all-done = bf16[8,16,4096]{2,1,0:T(8,128)(2,1)S(1)} async-done(((bf16[8,16,4096]{2,1,0:T(8,128)(2,1)}), bf16[8,16,4096]{2,1,0:T(8,128)(2,1)S(1)}, u32[]{:S(2)}, u32[]{:S(2)}) %all-to-all-start) | async-done | bytes 1048608 | tf_op jit(solution)/shard_map/all_to_all | solution.py:71
  45.3 0.0 copy-start.1
  45.3 3.0 %convolution_bitcast_fusion.5 = f32[2,128,256]{2,1,0:T(8,128)S(1)} fusion(bf16[128,4096,1]{1,0,2:T(8,128)(2,1)S(1)} %bitcast.52, bf16[2,4096,256]{2,1,0:T(8,128)(2,1)} %param.15), kind=kOutput, calls=%fused_computation.9 | convolution fusion | flops 536870912 | bytes 5505024 | tf_op jit(solution)/shard_map/rd,edh->erh/dot_general | solution.py:23
  48.4 0.0 copy-start
  48.4 0.4 copy-done.1
  48.8 0.8 fusion.5
  49.5 0.1 collective-permute-start
  49.6 1.1 %copy-done = bf16[2,1024,1024]{2,1,0:T(8,128)(2,1)S(1)} copy-done((bf16[2,1024,1024]{2,1,0:T(8,128)(2,1)S(1)}, bf16[2,1024,1024]{2,1,0:T(8,128)(2,1)}, u32[]{:S(2)}) %copy-start) | copy-done | bytes 4194328
  50.7 0.3 convolution_bitcast_fusion.3
  51.0 1.1 %collective-permute-done = bf16[2,128,256]{2,1,0:T(8,128)(2,1)S(1)} collective-permute-done((bf16[2,128,256]{2,1,0:T(8,128)(2,1)S(1)}, bf16[2,128,256]{2,1,0:T(8,128)(2,1)S(1)}, u32[]{:S(2)}, u32[]{:S(2)}) %collective-permute-start) | collective-permute-done | bytes 131104 | tf_op jit(solution)/shard_map/ppermute | solution.py:17
  52.1 1.9 %collective-permute-start.1 = (bf16[2,128,256]{2,1,0:T(8,128)(2,1)S(1)}, bf16[2,128,256]{2,1,0:T(8,128)(2,1)S(1)}, u32[]{:S(2)}, u32[]{:S(2)}) collective-permute-start(bf16[2,128,256]{2,1,0:T(8,128)(2,1)S(1)} %collective-permute-done), channel_id=1, source_target_pairs={{0,3},{1,0},{2,1},{3,2},{4,7},{5,4},{6,5},{7,6},{8,11},{9,8},{10,9... | collective-permute-start | bytes 393224 | tf_op jit(solution)/shard_map/ppermute | solution.py:17
  54.0 0.3 fusion
  54.3 2.2 %collective-permute-done.1 = bf16[2,128,256]{2,1,0:T(8,128)(2,1)S(1)} collective-permute-done((bf16[2,128,256]{2,1,0:T(8,128)(2,1)S(1)}, bf16[2,128,256]{2,1,0:T(8,128)(2,1)S(1)}, u32[]{:S(2)}, u32[]{:S(2)}) %collective-permute-start.1) | collective-permute-done | bytes 131104 | tf_op jit(solution)/shard_map/ppermute | solution.py:17
  56.5 1.9 %collective-permute-start.2 = (bf16[2,128,256]{2,1,0:T(8,128)(2,1)S(1)}, bf16[2,128,256]{2,1,0:T(8,128)(2,1)S(1)}, u32[]{:S(2)}, u32[]{:S(2)}) collective-permute-start(bf16[2,128,256]{2,1,0:T(8,128)(2,1)S(1)} %collective-permute-done.1), channel_id=1, source_target_pairs={{0,3},{1,0},{2,1},{3,2},{4,7},{5,4},{6,5},{7,6},{8,11},{9,8},{10,9... | collective-permute-start | bytes 393224 | tf_op jit(solution)/shard_map/ppermute | solution.py:17
  58.4 0.3 fusion.1
  58.7 2.2 %collective-permute-done.2 = bf16[2,128,256]{2,1,0:T(8,128)(2,1)S(1)} collective-permute-done((bf16[2,128,256]{2,1,0:T(8,128)(2,1)S(1)}, bf16[2,128,256]{2,1,0:T(8,128)(2,1)S(1)}, u32[]{:S(2)}, u32[]{:S(2)}) %collective-permute-start.2) | collective-permute-done | bytes 131104 | tf_op jit(solution)/shard_map/ppermute | solution.py:17
  60.9 0.3 fusion.2
  61.2 19.7 %all_to_all.15 = f32[8,16,1024]{2,1,0:T(8,128)S(1)} all-to-all(f32[8,16,1024]{2,1,0:T(8,128)S(1)} %bitcast.54), channel_id=1, replica_groups=mesh['ep'=8,'tp'=4] {'ep'}, dimensions={0} | all-to-all | bytes 1048576 | tf_op jit(solution)/shard_map/all_to_all | solution.py:80
  81.0 0.9 %fusion.6 = bf16[32,1024]{1,0:T(8,128)(2,1)} fusion(f32[8,16,1024]{2,1,0:T(8,128)S(1)} %all_to_all.15, s32[8,32]{1,0:T(8,128)S(1)} %copy.22, pred[8,32]{1,0:T(8,128)(4,1)S(1)} %bitcast.57), kind=kOutput, calls=%fused_computation.14 | convolution fusion | flops 50372608 | bytes 591104 | tf_op jit(solution)/shard_map/psr,psd->rd/dot_general | solution.py:87
  (6 shorter events, 0.0 us)
Async XLA Ops:
  3.1 13.8 %all-to-all-start.1 = ((f32[8,16,2]{1,2,0:T(2,128)}), f32[8,16,2]{1,2,0:T(2,128)S(1)}, u32[]{:S(2)}, u32[]{:S(2)}) async-start(f32[8,16,2]{1,2,0:T(2,128)} %fusion.20), calls=%async_computation.1 | async-start | bytes 16384 | tf_op jit(solution)/shard_map/all_to_all | solution.py:72
  16.9 28.5 %all-to-all-start = ((bf16[8,16,4096]{2,1,0:T(8,128)(2,1)}), bf16[8,16,4096]{2,1,0:T(8,128)(2,1)S(1)}, u32[]{:S(2)}, u32[]{:S(2)}) async-start(bf16[8,16,4096]{2,1,0:T(8,128)(2,1)} %convolution_convert_fusion), calls=%async_computation | async-start | bytes 2097152 | tf_op jit(solution)/shard_map/all_to_all | solution.py:71
  45.3 3.4 %copy-start.1 = (bf16[2,4096,256]{2,1,0:T(8,128)(2,1)S(1)}, bf16[2,4096,256]{2,1,0:T(8,128)(2,1)}, u32[]{:S(2)}) copy-start(bf16[2,4096,256]{2,1,0:T(8,128)(2,1)} %param.16) | copy-start | bytes 12582916
  48.4 2.3 %copy-start = (bf16[2,1024,1024]{2,1,0:T(8,128)(2,1)S(1)}, bf16[2,1024,1024]{2,1,0:T(8,128)(2,1)}, u32[]{:S(2)}) copy-start(bf16[2,1024,1024]{2,1,0:T(8,128)(2,1)} %param.17) | copy-start | bytes 12582916
  49.5 2.6 %collective-permute-start = (bf16[2,128,256]{2,1,0:T(8,128)(2,1)S(1)}, bf16[2,128,256]{2,1,0:T(8,128)(2,1)S(1)}, u32[]{:S(2)}, u32[]{:S(2)}) collective-permute-start(bf16[2,128,256]{2,1,0:T(8,128)(2,1)S(1)} %fusion.5), channel_id=1, source_target_pairs={{0,3},{1,0},{2,1},{3,2},{4,7},{5,4},{6,5},{7,6},{8,11},{9,8},{10,9... | collective-permute-start | bytes 393224 | tf_op jit(solution)/shard_map/ppermute | solution.py:17
  52.1 4.4 %collective-permute-start.1 = (bf16[2,128,256]{2,1,0:T(8,128)(2,1)S(1)}, bf16[2,128,256]{2,1,0:T(8,128)(2,1)S(1)}, u32[]{:S(2)}, u32[]{:S(2)}) collective-permute-start(bf16[2,128,256]{2,1,0:T(8,128)(2,1)S(1)} %collective-permute-done), channel_id=1, source_target_pairs={{0,3},{1,0},{2,1},{3,2},{4,7},{5,4},{6,5},{7,6},{8,11},{9,8},{10,9... | collective-permute-start | bytes 393224 | tf_op jit(solution)/shard_map/ppermute | solution.py:17
  56.5 4.4 %collective-permute-start.2 = (bf16[2,128,256]{2,1,0:T(8,128)(2,1)S(1)}, bf16[2,128,256]{2,1,0:T(8,128)(2,1)S(1)}, u32[]{:S(2)}, u32[]{:S(2)}) collective-permute-start(bf16[2,128,256]{2,1,0:T(8,128)(2,1)S(1)} %collective-permute-done.1), channel_id=1, source_target_pairs={{0,3},{1,0},{2,1},{3,2},{4,7},{5,4},{6,5},{7,6},{8,11},{9,8},{10,9... | collective-permute-start | bytes 393224 | tf_op jit(solution)/shard_map/ppermute | solution.py:17
